TPU v7x, 32 devices: a whole 2x2x4 slice. The times are simulated.
32 devices in a mesh: rep: 2 (over y), fs: 4 (over z), tp: 4 (over x, core).
Axes of the slice: x: 2, y: 2, z: 4, core: 2. Of those that a mesh axis runs over, the one named last changes fastest.
Arguments:
- tokens: bfloat16 [4096, 2048], P(('rep', 'fs')), may hold values from -6 to 6
- norm_gain: float32 [2048], replicated, may hold values from 0.1 to 1.9
- up_weight: bfloat16 [2048, 4096], P('fs', 'tp'), may hold values from -0.125 to 0.125
- down_weight: bfloat16 [4096, 2048], P('tp', 'fs'), may hold values from -0.09375 to 0.09375
Outputs:
- result: bfloat16 [4096, 2048], P(('rep', 'fs', 'tp'))
All inputs are finite; a program needn't handle non-finite values.
Results may differ from a plain program's by a relative error of at most 0.012.
Values may be sent and summed in bfloat16 or wider, within the bound.
A program may use at most 64 MiB of HBM per device.

v0:
```python
import jax
import jax.numpy as jnp
from jax import lax
from jax.sharding import PartitionSpec as P

EPS = 1e-06


def shards(tokens, norm_gain, up_weight, down_weight):
    xf = tokens.astype(jnp.float32)
    scale = lax.rsqrt(jnp.mean(xf * xf, axis=-1, keepdims=True) + EPS)
    normed = (xf * scale * norm_gain).astype(jnp.bfloat16)
    rows = tokens.shape[0]
    halves = lax.axis_size("rep")
    share = up_weight.shape[0] // halves
    mine = lax.dynamic_slice_in_dim(up_weight, lax.axis_index("rep") * share, share, 0)
    arranged = normed.reshape(rows, -1, halves, share).transpose(0, 2, 1, 3).reshape(rows, -1)
    lifted = jnp.dot(
        arranged,
        lax.all_gather(mine, ("rep", "fs"), axis=0, tiled=True),
        preferred_element_type=jnp.float32,
    )
    width = down_weight.shape[1] // halves
    down_mine = lax.dynamic_slice_in_dim(down_weight, lax.axis_index("rep") * width, width, 1)
    collected = lax.all_gather(down_mine, ("rep", "fs"), axis=1, tiled=True)
    hidden_rows = collected.shape[0]
    down_block = (
        collected.reshape(hidden_rows, halves, -1, width)
        .transpose(0, 2, 1, 3)
        .reshape(hidden_rows, -1)
    )
    hidden = jnp.square(jnp.maximum(lifted, 0.0)).astype(jnp.bfloat16)
    own_rows = rows // lax.axis_size("tp")
    summed = lax.psum_scatter(
        jnp.dot(hidden, down_block, preferred_element_type=jnp.float32).astype(jnp.bfloat16),
        "tp",
        scatter_dimension=0,
        tiled=True,
    ).astype(jnp.float32)
    residual = lax.dynamic_slice_in_dim(xf, lax.axis_index("tp") * own_rows, own_rows, 0)
    return (residual + summed).astype(jnp.bfloat16)


def solution(mesh):
    placed = (P(("rep", "fs"), None), P(), P("fs", "tp"), P("tp", "fs"))
    return jax.shard_map(
        shards, mesh=mesh, in_specs=placed, out_specs=P(("rep", "fs", "tp"), None), check_vma=False
    )
```

profile of v0, /device:TPU:0, one launch (start us, length us, event | category | flops | bytes accessed | tf_op | source)
XLA Modules:
  0.0 208.4 jit_solution(14472330394279281038)
XLA Ops:
  6.5 0.0 copy-start
  6.5 0.0 copy-start.1
  6.5 0.0 copy-start.2
  6.5 0.0 all-gather.5.cloned.1.call-start
  6.6 1.2 copy-done
  7.8 0.8 constant_dynamic-slice_fusion
  8.6 2.1 copy.9
  10.6 0.0 all-gather.5.cloned.1.call-update
  10.7 0.0 all-gather.3.cloned.1.call-start
  10.7 1.9 constant_dynamic-slice_fusion.1
  12.6 0.0 all-gather.3.cloned.1.call-update
  12.6 0.0 reduce-scatter.2.cloned.1.call-start
  12.7 0.0 copy-done.1
  12.7 0.5 multiply_reduce_fusion
  13.2 0.0 copy-done.2
  13.2 1.9 multiply_convert_fusion
  15.1 4.5 %reshape.21 = bf16[512,4,2,256]{3,2,1,0:T(2,128)(2,1)} reshape(bf16[512,2048]{1,0:T(8,128)(2,1)} %multiply_convert_fusion) | data formatting | bytes 4194304 | tf_op jit(solution)/shard_map/reshape | solution.py:17
  19.6 6.2 %copy.6 = bf16[512,4,2,256]{0,3,1,2:T(8,128)(2,1)} copy(bf16[512,4,2,256]{3,2,1,0:T(2,128)(2,1)} %reshape.21) | data formatting | bytes 4194304 | tf_op jit(solution)/shard_map/reshape | solution.py:17
  25.7 60.6 %all-gather.5.cloned.1.call-done = bf16[1024,2048]{0,1:T(8,128)(2,1)} async-done(((bf16[1024,256]{0,1:T(8,128)(2,1)}), bf16[1024,2048]{0,1:T(8,128)(2,1)}) %all-gather.5.cloned.1.call-update) | async-done | bytes 4194320 | tf_op jit(solution)/shard_map/all_gather | solution.py:25
  86.3 4.6 %copy.8 = bf16[1024,4,2,256]{0,3,2,1:T(8,128)(2,1)} copy(bf16[1024,4,2,256]{0,3,1,2:T(8,128)(2,1)} %bitcast.10) | data formatting | bytes 8388608 | tf_op jit(solution)/shard_map/transpose | solution.py:29
  90.9 68.9 %all-gather.3.cloned.1.call-done = bf16[2048,1024]{1,0:T(8,128)(2,1)} async-done(((bf16[256,1024]{1,0:T(8,128)(2,1)}), bf16[2048,1024]{1,0:T(8,128)(2,1)}) %all-gather.3.cloned.1.call-update) | async-done | bytes 4194320 | tf_op jit(solution)/shard_map/all_gather | solution.py:20
  159.8 9.9 %convolution_convert_fusion = bf16[512,2048]{1,0:T(8,128)(2,1)} fusion(bf16[1024,2048]{0,1:T(8,128)(2,1)} %bitcast.11, bf16[512,2048]{0,1:T(8,128)(2,1)} %bitcast.12, bf16[2048,1024]{1,0:T(8,128)(2,1)} %all-gather.3.cloned.1.call-done), kind=kOutput, calls=%fused_computation.2 | convolution fusion | flops 4297588736 | bytes 12582912 | tf_op jit(solution)/shard_map/dot_general | solution.py:35
  169.7 0.0 reduce-scatter.2.cloned.1.call-update
  169.8 2.5 %convert_element_type.18 = f32[512,2048]{1,0:T(8,128)} convert(bf16[512,2048]{1,0:T(8,128)(2,1)S(1)} %copy-done.1) | non-fusion elementwise | flops 1048576 | bytes 6291456 | tf_op jit(solution)/shard_map/convert_element_type | solution.py:10
  172.2 27.4 %reduce-scatter.2.cloned.1.call-done = bf16[128,2048]{1,0:T(8,128)(2,1)} async-done(((bf16[512,2048]{1,0:T(8,128)(2,1)}), bf16[128,2048]{1,0:T(8,128)(2,1)}) %reduce-scatter.2.cloned.1.call-update) | async-done | bytes 524304 | tf_op jit(solution)/shard_map/reduce_scatter | solution.py:34
  199.6 2.3 %add_convert_fusion = bf16[128,2048]{1,0:T(8,128)(2,1)} fusion(bf16[128,2048]{1,0:T(8,128)(2,1)} %reduce-scatter.2.cloned.1.call-done, f32[512,2048]{1,0:T(8,128)} %convert_element_type.18, s32[]{:T(128)S(6)} %select_n.7), kind=kLoop, calls=%fused_computation.4 | loop fusion | flops 786432 | bytes 2097156 | tf_op jit(solution)/shard_map/convert_element_type | solution.py:41
  (1 shorter events, 0.0 us)
Async XLA Ops:
  6.5 1.2 copy-start
  6.5 6.1 %copy-start.1 = (bf16[512,2048]{1,0:T(8,128)(2,1)S(1)}, bf16[512,2048]{1,0:T(8,128)(2,1)}, u32[]{:S(2)}) copy-start(bf16[512,2048]{1,0:T(8,128)(2,1)} %param.4) | copy-start | bytes 6291460
  6.5 6.6 %copy-start.2 = (f32[2048]{0:T(1024)S(1)}, f32[2048]{0:T(1024)}, u32[]{:S(2)}) copy-start(f32[2048]{0:T(1024)} %param.5) | copy-start | bytes 24580
  6.5 79.8 %all-gather.5.cloned.1.call-start = ((), (), s32[]{:S(2)}) async-start(), calls=%async_computation.2 | async-start | bytes 4718592 | tf_op jit(solution)/shard_map/all_gather | solution.py:25
  10.7 149.2 %all-gather.3.cloned.1.call-start = ((), (), s32[]{:S(2)}) async-start(), calls=%async_computation.1 | async-start | bytes 4718592 | tf_op jit(solution)/shard_map/all_gather | solution.py:20
  12.6 187.0 %reduce-scatter.2.cloned.1.call-start = ((), (), s32[]{:S(2)}) async-start(), calls=%async_computation.3 | async-start | bytes 2621440 | tf_op jit(solution)/shard_map/reduce_scatter | solution.py:34
Sparse Core Ops, SparseCore 0:
  10.8 75.4 all-gather.4
  88.5 71.3 all-gather.2
  169.9 29.6 reduce-scatter.1
where the time goes:
time: 209 us; the launch traced here: 208 us
  waiting for transfers between devices  157 us (75%)
  local copies, waits for them, and re-layouts  21.2 us (10%)
  between operations  13.1 us (6%)
  matrix products  9.9 us (5%)
  other arithmetic  7.13 us (3%)
    all_gather x1, waiting for transfers between devices, shards(): lax.all_gather(mine, ('rep', 'fs'), axis=0, tiled=True)  68.9 us
    all_gather x1, waiting for transfers between devices, shards(): collected = lax.all_gather(down_mine, ('rep', 'fs'), axis=1, tiled=True)  60.6 us
    reduce_scatter x1, waiting for transfers between devices, shards(): lax.psum_scatter(jnp.dot(hidden, down_block, preferred_element_type=jnp.f...  27.4 us
    reshape x2, local copies, waits for them, and re-layouts, shards(): normed.reshape(rows, -1, halves, share).transpose(0, 2, 1, 3)  10.7 us
    dot_general x1, matrix products, shards(): jnp.dot(hidden, down_block, preferred_element_type=jnp.float32)  9.9 us
    transpose x1, local copies, waits for them, and re-layouts, shards(): down_block = collected.reshape(hidden_rows, halves, -1, width).transpose(...  4.59 us
  transfers between devices with their start and end apart: 3, of which 3 were waited for; matrix products, arithmetic and copies ran while one was open for 11% of the time, Pallas kernels for 0%

commit v1 on v0

--- a/solution.py
+++ b/solution.py
@@ -17,7 +17,10 @@
     arranged = normed.reshape(rows, -1, halves, share).transpose(0, 2, 1, 3).reshape(rows, -1)
     lifted = jnp.dot(
         arranged,
-        lax.all_gather(mine, ("rep", "fs"), axis=0, tiled=True),
+        jnp.concatenate(
+            lax.all_to_all(jnp.stack([mine] * lax.axis_size(("rep", "fs"))), ("rep", "fs"), 0, 0),
+            axis=0,
+        ),
         preferred_element_type=jnp.float32,
     )
     width = down_weight.shape[1] // halves

time: 209 us -> 213 us (1.019)
  starting transfers between devices: 0.09 us -> 7.48 us
  waiting for transfers between devices: 157 us -> 154 us
    all_gather x1 -> x0, waiting for transfers between devices: 68.9 us -> none  [shards(): lax.all_gather(mine, ('rep', 'fs'), axis=0, tiled=True)]
    all_gather x1, waiting for transfers between devices: 60.6 us -> 127 us  [shards(): collected = lax.all_gather(down_mine, ('rep', 'fs'), axis=1, tiled=True)]
    all_to_all x0 -> x1, starting transfers between devices: none -> 7.44 us  [shards(): lax.all_to_all(jnp.stack([mine] * lax.axis_size(('rep', 'fs'))), ('rep',...]
    another operation x0 -> x1, local copies, waits for them, and re-layouts: none -> 2.49 us  [shards(): jnp.stack([mine] * lax.axis_size(('rep', 'fs')))]
where the time goes in v1:
time: 213 us
  waiting for transfers between devices  154 us (72%)
  local copies, waits for them, and re-layouts  21 us (10%)
  between operations  13.4 us (6%)
  matrix products  9.91 us (5%)
  starting transfers between devices  7.48 us (4%)
  other arithmetic  7.11 us (3%)
    all_gather x1, waiting for transfers between devices, shards(): collected = lax.all_gather(down_mine, ('rep', 'fs'), axis=1, tiled=True)  127 us
    reduce_scatter x1, waiting for transfers between devices, shards(): lax.psum_scatter(jnp.dot(hidden, down_block, preferred_element_type=jnp.f...  26.3 us
    reshape x2, local copies, waits for them, and re-layouts, shards(): normed.reshape(rows, -1, halves, share).transpose(0, 2, 1, 3)  10.6 us
    dot_general x1, matrix products, shards(): jnp.dot(hidden, down_block, preferred_element_type=jnp.float32)  9.91 us
    all_to_all x1, starting transfers between devices, shards(): lax.all_to_all(jnp.stack([mine] * lax.axis_size(('rep', 'fs'))), ('rep',...  7.44 us
    transpose x1, local copies, waits for them, and re-layouts, shards(): down_block = collected.reshape(hidden_rows, halves, -1, width).transpose(...  4.57 us
  transfers between devices with their start and end apart: 3, of which 3 were waited for; matrix products, arithmetic and copies ran while one was open for 11% of the time, Pallas kernels for 0%

profile of v1, /device:TPU:0, one launch (start us, length us, event | category | flops | bytes accessed | tf_op | source)
XLA Modules:
  0.0 212.8 jit_solution(5442473745013737365)
XLA Ops:
  6.5 0.0 copy-start
  6.5 0.0 all-gather.2.cloned.1.call-start
  6.5 1.2 copy-done
  7.8 1.0 copy.9
  8.8 0.0 all-gather.2.cloned.1.call-update
  8.8 1.1 constant_dynamic-slice_fusion.1
  9.9 2.5 %stack.2 = bf16[8,256,1024]{2,1,0:T(8,128)(2,1)} broadcast(bf16[256,1024]{1,0:T(8,128)(2,1)S(1)} %constant_dynamic-slice_fusion.1), dimensions={1,2} | broadcast | bytes 4718592 | tf_op jit(solution)/shard_map/stack | solution.py:21
  12.4 0.0 copy-start.1
  12.4 0.0 copy-start.2
  12.4 7.4 %all-to-all-start = ((bf16[8,256,1024]{2,1,0:T(8,128)(2,1)}), bf16[8,256,1024]{2,1,0:T(8,128)(2,1)}, u32[]{:S(2)}, u32[]{:S(2)}) async-start(bf16[8,256,1024]{2,1,0:T(8,128)(2,1)} %stack.2), calls=%async_computation | async-start | bytes 8388608 | tf_op jit(solution)/shard_map/all_to_all | solution.py:21
  19.9 0.0 reduce-scatter.2.cloned.1.call-start
  19.9 0.0 copy-done.1
  19.9 0.5 multiply_reduce_fusion
  20.4 0.0 copy-done.2
  20.4 1.9 multiply_convert_fusion
  22.3 4.5 %reshape.26 = bf16[512,4,2,256]{3,2,1,0:T(2,128)(2,1)} reshape(bf16[512,2048]{1,0:T(8,128)(2,1)} %multiply_convert_fusion) | data formatting | bytes 4194304 | tf_op jit(solution)/shard_map/reshape | solution.py:17
  26.8 6.1 %copy.6 = bf16[512,4,2,256]{0,3,1,2:T(8,128)(2,1)} copy(bf16[512,4,2,256]{3,2,1,0:T(2,128)(2,1)} %reshape.26) | data formatting | bytes 4194304 | tf_op jit(solution)/shard_map/reshape | solution.py:17
  32.9 126.8 %all-gather.2.cloned.1.call-done = bf16[1024,2048]{0,1:T(8,128)(2,1)} async-done(((bf16[1024,256]{0,1:T(8,128)(2,1)}), bf16[1024,2048]{0,1:T(8,128)(2,1)}) %all-gather.2.cloned.1.call-update) | async-done | bytes 4194320 | tf_op jit(solution)/shard_map/all_gather | solution.py:28
  159.7 4.6 %copy.8 = bf16[1024,4,2,256]{0,3,2,1:T(8,128)(2,1)} copy(bf16[1024,4,2,256]{0,3,1,2:T(8,128)(2,1)} %bitcast.11) | data formatting | bytes 8388608 | tf_op jit(solution)/shard_map/transpose | solution.py:32
  164.3 0.7 all-to-all-done
  164.9 9.9 %convolution_convert_fusion = bf16[512,2048]{1,0:T(8,128)(2,1)} fusion(bf16[1024,2048]{0,1:T(8,128)(2,1)} %bitcast.12, bf16[512,2048]{0,1:T(8,128)(2,1)} %bitcast.13, bf16[2048,1024]{1,0:T(8,128)(2,1)} %bitcast.2), kind=kOutput, calls=%fused_computation.2 | convolution fusion | flops 4297588736 | bytes 12582912 | tf_op jit(solution)/shard_map/dot_general | solution.py:38
  174.8 0.0 reduce-scatter.2.cloned.1.call-update
  174.9 2.5 %convert_element_type.18 = f32[512,2048]{1,0:T(8,128)} convert(bf16[512,2048]{1,0:T(8,128)(2,1)S(1)} %copy-done.1) | non-fusion elementwise | flops 1048576 | bytes 6291456 | tf_op jit(solution)/shard_map/convert_element_type | solution.py:10
  177.3 26.3 %reduce-scatter.2.cloned.1.call-done = bf16[128,2048]{1,0:T(8,128)(2,1)} async-done(((bf16[512,2048]{1,0:T(8,128)(2,1)}), bf16[128,2048]{1,0:T(8,128)(2,1)}) %reduce-scatter.2.cloned.1.call-update) | async-done | bytes 524304 | tf_op jit(solution)/shard_map/reduce_scatter | solution.py:37
  203.7 2.3 %add_convert_fusion = bf16[128,2048]{1,0:T(8,128)(2,1)} fusion(bf16[128,2048]{1,0:T(8,128)(2,1)} %reduce-scatter.2.cloned.1.call-done, f32[512,2048]{1,0:T(8,128)} %convert_element_type.18, s32[]{:T(128)S(6)} %select_n.7), kind=kLoop, calls=%fused_computation.4 | loop fusion | flops 786432 | bytes 2097156 | tf_op jit(solution)/shard_map/convert_element_type | solution.py:44
  (2 shorter events, 0.0 us)
Async XLA Ops:
  6.5 1.2 copy-start
  6.5 153.2 %all-gather.2.cloned.1.call-start = ((), (), s32[]{:S(2)}) async-start(), calls=%async_computation.2 | async-start | bytes 4718592 | tf_op jit(solution)/shard_map/all_gather | solution.py:28
  12.4 7.5 %copy-start.1 = (bf16[512,2048]{1,0:T(8,128)(2,1)S(1)}, bf16[512,2048]{1,0:T(8,128)(2,1)}, u32[]{:S(2)}) copy-start(bf16[512,2048]{1,0:T(8,128)(2,1)} %param.4) | copy-start | bytes 6291460
  12.4 8.0 %copy-start.2 = (f32[2048]{0:T(1024)S(1)}, f32[2048]{0:T(1024)}, u32[]{:S(2)}) copy-start(f32[2048]{0:T(1024)} %param.5) | copy-start | bytes 24580
  12.4 152.5 %all-to-all-start = ((bf16[8,256,1024]{2,1,0:T(8,128)(2,1)}), bf16[8,256,1024]{2,1,0:T(8,128)(2,1)}, u32[]{:S(2)}, u32[]{:S(2)}) async-start(bf16[8,256,1024]{2,1,0:T(8,128)(2,1)} %stack.2), calls=%async_computation | async-start | bytes 8388608 | tf_op jit(solution)/shard_map/all_to_all | solution.py:21
  19.9 183.8 %reduce-scatter.2.cloned.1.call-start = ((), (), s32[]{:S(2)}) async-start(), calls=%async_computation.3 | async-start | bytes 2621440 | tf_op jit(solution)/shard_map/reduce_scatter | solution.py:37
Sparse Core Ops, SparseCore 0:
  9.5 150.1 all-gather.1
  175.0 28.6 reduce-scatter.1
